TPU v7x, 256 devices: a 2x2x32 block of a 4x8x32 slice. The times are simulated.
256 devices in a mesh: grp: 4 (over y, x), ep: 32 (over z), tp: 2 (over core).
Axes of the slice: x: 2, y: 2, z: 32, core: 2. Of those that a mesh axis runs over, the one named last changes fastest.
The devices are a block of a 4x8x32 slice.
Arguments:
- tokens: bfloat16 [65536, 2048], P(('grp', 'ep', 'tp')), parts along dimension 0, may hold values from -6 to 6
- norm_gain: float32 [2048], replicated, may hold values from 0.1 to 1.9
- expert_ids: int32 [65536, 2], P(('grp', 'ep', 'tp')), parts along dimension 0, may hold values from 0 to 31, all different within a row; in each aligned block of 256 rows (0 to 255, 256 to 511, ...) at most 24 rows name the same one
- route_weights: float32 [65536, 2], P(('grp', 'ep', 'tp')), parts along dimension 0, may hold values from 0.05 to 1
- w_gate: bfloat16 [32, 2048, 1024], P('ep', None, 'tp'), may hold values from -0.125 to 0.125
- w_up: bfloat16 [32, 2048, 1024], P('ep', None, 'tp'), may hold values from -0.125 to 0.125
- w_down: bfloat16 [32, 1024, 2048], P('ep', 'tp'), may hold values from -0.1875 to 0.1875
Outputs:
- mixed: bfloat16 [65536, 2048], P(('grp', 'ep', 'tp')), parts along dimension 0
There are 4 independent parts, one for each index of `grp`. A program takes and returns all parts, laid end to end along the dimension named above; an argument that names none is the same for every part. Nothing has to cross between parts.
Inputs may be any that keep to these rules, and one draw needn't show every extreme that they name: `expert_ids`: each row names 2 different experts. Among the rows of one device no expert is named more than 24 times, and in every draw some expert is named exactly 24 times by the rows of some device.
All inputs are finite; a program needn't handle non-finite values.
Results may differ from a plain program's by a relative error of at most 0.0071.
Values may be sent and summed in bfloat16 or wider, within the bound.
A program may use at most 128 MiB of HBM per device.

v0:
```python
import jax
import jax.numpy as jnp
from jax import lax
from jax.sharding import PartitionSpec as P


def in_one_piece(arrays, axis, dim, along):
    ends, at = ([], 0)
    for a in arrays[:-1]:
        at += a.shape[along]
        ends.append(at)
    both = jnp.concatenate(arrays, axis=along)
    return tuple(jnp.split(lax.all_gather(both, axis, axis=dim, tiled=True), ends, axis=along))


def per_device(tokens, norm_gain, expert_ids, route_weights, w_gate, w_up, w_down):
    tok_rows = tokens.shape[0]
    top_count = expert_ids.shape[1]
    width = tokens.shape[1]
    local_experts = w_gate.shape[0]
    ep_size = lax.axis_size("ep")
    experts = local_experts * ep_size
    slots = 3 * tok_rows * top_count // (2 * experts)
    values = tokens.astype(jnp.float32)
    scale = lax.rsqrt(jnp.mean(values * values, axis=-1, keepdims=True) + 1e-06)
    normed = (values * scale * norm_gain).astype(jnp.bfloat16)
    flat_ids = expert_ids.reshape(-1)
    onehot = (flat_ids[:, None] == jnp.arange(experts, dtype=jnp.int32)[None, :]).astype(jnp.int32)
    before = jnp.cumsum(onehot, axis=0) - onehot
    slot_of = jnp.sum(before * onehot, axis=1)
    target = flat_ids * slots + slot_of
    owner = jnp.arange(tok_rows * top_count, dtype=jnp.int32) // top_count + 1
    source = jnp.zeros((experts * slots,), jnp.int32).at[target].set(owner)
    filled = source > 0
    picked = jnp.take(normed, jnp.maximum(source - 1, 0), axis=0)
    outgoing = jnp.where(filled[:, None], picked, jnp.zeros_like(picked))
    outgoing = outgoing.reshape(ep_size, local_experts, slots, width)
    gate_full, up_full = in_one_piece((w_gate, w_up), "tp", 2, 0)
    down_full = lax.all_gather(w_down, "tp", axis=1, tiled=True)
    arrived = lax.all_to_all(outgoing, "ep", split_axis=0, concat_axis=0, tiled=True)
    senders, _, part_slots, _ = arrived.shape
    rows = jnp.transpose(arrived, (1, 0, 2, 3)).reshape(local_experts, senders * part_slots, width)
    gate = jnp.einsum("erd,edf->erf", rows, gate_full, preferred_element_type=jnp.float32)
    upper = jnp.einsum("erd,edf->erf", rows, up_full, preferred_element_type=jnp.float32)
    hidden = (jax.nn.silu(gate) * upper).astype(jnp.bfloat16)
    result = jnp.einsum(
        "erf,efd->erd", hidden, down_full, preferred_element_type=jnp.float32
    ).astype(jnp.bfloat16)
    result = result.reshape(local_experts, senders, part_slots, width)
    result = jnp.transpose(result, (1, 0, 2, 3))
    results = lax.all_to_all(result, "ep", split_axis=0, concat_axis=0, tiled=True)
    results = results.reshape(experts * slots, width)
    gathered = jnp.take(results, target, axis=0).reshape(tok_rows, top_count, width)
    mixed = jnp.sum(route_weights[:, :, None] * gathered.astype(jnp.float32), axis=1)
    return mixed.astype(jnp.bfloat16)


def solution(mesh):
    in_specs = (
        P(("grp", "ep", "tp"), None),
        P(),
        P(("grp", "ep", "tp"), None),
        P(("grp", "ep", "tp"), None),
        P("ep", None, "tp"),
        P("ep", None, "tp"),
        P("ep", "tp", None),
    )
    out_specs = P(("grp", "ep", "tp"), None)
    return jax.shard_map(
        per_device, mesh=mesh, in_specs=in_specs, out_specs=out_specs, check_vma=False
    )
```

profile of v0, /device:TPU:46, one launch (start us, length us, event | category | flops | bytes accessed | tf_op | source)
XLA Modules:
  0.0 665.8 jit_solution(12743148507947471114)
XLA Ops:
  6.5 0.8 copy.23
  7.4 0.1 eq.26
  7.5 0.1 reshape.138
  7.7 0.7 broadcast_multiply_fusion
  8.4 1.2 reduce-window.6
  9.5 0.2 slice_reduce_fusion
  9.8 0.1 copy.28
  9.9 0.1 mul.62
  10.1 0.1 fusion.12
  10.2 2.4 scatter_custom_fusion
  12.7 0.1 broadcast_in_dim.44
  12.8 0.1 broadcast_in_dim.46
  12.9 1.5 fusion.7
  14.4 1.5 fusion.9
  16.0 4.3 gather_fusion
  20.2 3.3 select_select_fusion
  23.6 32.7 %all-to-all-start = ((bf16[32,1,24,2048]{3,2,1,0:T(8,128)(2,1)}), bf16[32,1,24,2048]{3,2,1,0:T(8,128)(2,1)S(1)}, u32[]{:S(2)}, u32[]{:S(2)}) async-start(bf16[32,1,24,2048]{3,2,1,0:T(8,128)(2,1)} %select_select_fusion), calls=%async_computation | async-start | bytes 6291456 | tf_op jit(solution)/shard_map/all_to_all | solution.py:40
  56.3 4.6 pad_maximum_fusion
  61.0 0.7 all-gather.5.cloned.1.call-update
  61.7 36.7 %all-gather.3.cloned.1.call-done = bf16[2,2048,1024]{2,1,0:T(8,128)(2,1)} async-done(((bf16[2,2048,512]{2,1,0:T(8,128)(2,1)}), bf16[2,2048,1024]{2,1,0:T(8,128)(2,1)}) %all-gather.3.cloned.1.call-update) | async-done | bytes 8388624 | tf_op jit(solution)/shard_map/all_gather | solution.py:13
  98.5 233.4 %all-to-all-done = bf16[32,1,24,2048]{3,2,1,0:T(8,128)(2,1)S(1)} async-done(((bf16[32,1,24,2048]{3,2,1,0:T(8,128)(2,1)}), bf16[32,1,24,2048]{3,2,1,0:T(8,128)(2,1)S(1)}, u32[]{:S(2)}, u32[]{:S(2)}) %all-to-all-start) | async-done | bytes 3145760 | tf_op jit(solution)/shard_map/all_to_all | solution.py:40
  331.8 5.3 fusion
  337.2 5.0 multiply_convert_fusion
  342.2 7.7 %fusion.4 = bf16[768,2048]{1,0:T(8,128)(2,1)} fusion(bf16[768,1024]{1,0:T(8,128)(2,1)} %multiply_convert_fusion, bf16[1,1024,2048]{2,1,0:T(8,128)(2,1)} %all-gather.5.cloned.1.call-done), kind=kOutput, calls=%fused_computation.12 | convolution fusion | flops 3222798336 | bytes 8912896 | tf_op jit(solution)/shard_map/erf,efd->erd/dot_general | solution.py:46
  350.0 17.5 %all-to-all-start.1 = ((bf16[32,1,24,2048]{3,2,1,0:T(8,128)(2,1)}), bf16[32,1,24,2048]{3,2,1,0:T(8,128)(2,1)S(1)}, u32[]{:S(2)}, u32[]{:S(2)}) async-start(bf16[32,1,24,2048]{3,2,1,0:T(8,128)(2,1)} %bitcast.49), calls=%async_computation.1 | async-start | bytes 6291456 | tf_op jit(solution)/shard_map/all_to_all | solution.py:51
  367.5 0.1 reduce_sum.32
  367.7 0.2 copy.27
  367.9 0.1 copy.22
  368.1 275.1 %all-to-all-done.1 = bf16[32,1,24,2048]{3,2,1,0:T(8,128)(2,1)S(1)} async-done(((bf16[32,1,24,2048]{3,2,1,0:T(8,128)(2,1)}), bf16[32,1,24,2048]{3,2,1,0:T(8,128)(2,1)S(1)}, u32[]{:S(2)}, u32[]{:S(2)}) %all-to-all-start.1) | async-done | bytes 3145760 | tf_op jit(solution)/shard_map/all_to_all | solution.py:51
  643.2 3.3 gather_fusion.1
  646.5 3.2 gather.15
  649.7 9.2 %multiply_reduce_fusion = bf16[256,2048]{1,0:T(8,128)(2,1)} fusion(bf16[256,2,2048]{2,1,0:T(2,128)(2,1)S(1)} %gather.15, pred[256,2]{1,0:T(8,128)(4,1)S(1)} %copy.27, f32[256,2]{1,0:T(8,128)S(1)} %copy.22), kind=kLoop, calls=%fused_computation.10 | loop fusion | flops 3670016 | bytes 3148288 | tf_op jit(solution)/shard_map/reduce_sum | solution.py:54
  (22 shorter events, 0.4 us)
Async XLA Ops:
  23.6 308.3 %all-to-all-start = ((bf16[32,1,24,2048]{3,2,1,0:T(8,128)(2,1)}), bf16[32,1,24,2048]{3,2,1,0:T(8,128)(2,1)S(1)}, u32[]{:S(2)}, u32[]{:S(2)}) async-start(bf16[32,1,24,2048]{3,2,1,0:T(8,128)(2,1)} %select_select_fusion), calls=%async_computation | async-start | bytes 6291456 | tf_op jit(solution)/shard_map/all_to_all | solution.py:40
  56.2 42.2 %all-gather.3.cloned.1.call-start = ((), (), s32[]{:S(2)}) async-start(), calls=%async_computation.2 | async-start | bytes 12582912 | tf_op jit(solution)/shard_map/all_gather | solution.py:13
  60.9 281.3 %all-gather.5.cloned.1.call-start = ((), (), s32[]{:S(2)}) async-start(), calls=%async_computation.3 | async-start | bytes 6291456 | tf_op jit(solution)/shard_map/all_gather | solution.py:39
  331.8 5.4 copy-start.2
  350.0 17.7 %copy-start = (s32[256,2]{0,1:T(2,128)S(1)}, s32[256,2]{0,1:T(2,128)}, u32[]{:S(2)}) copy-start(s32[256,2]{0,1:T(2,128)} %param.9) | copy-start | bytes 6148
  350.0 17.9 %copy-start.1 = (f32[256,2]{0,1:T(2,128)S(1)}, f32[256,2]{0,1:T(2,128)}, u32[]{:S(2)}) copy-start(f32[256,2]{0,1:T(2,128)} %param.10) | copy-start | bytes 6148
  350.0 293.2 %all-to-all-start.1 = ((bf16[32,1,24,2048]{3,2,1,0:T(8,128)(2,1)}), bf16[32,1,24,2048]{3,2,1,0:T(8,128)(2,1)S(1)}, u32[]{:S(2)}, u32[]{:S(2)}) async-start(bf16[32,1,24,2048]{3,2,1,0:T(8,128)(2,1)} %bitcast.49), calls=%async_computation.1 | async-start | bytes 6291456 | tf_op jit(solution)/shard_map/all_to_all | solution.py:51
Sparse Core Ops, SparseCore 0:
  61.1 37.3 all-gather.2
  100.3 31.8 all-gather.4
where the time goes:
time: 671 us; the launch traced here: 666 us
  waiting for transfers between devices  546 us (81%)
  starting transfers between devices  50.3 us (7%)
  other arithmetic  22.2 us (3%)
  matrix products  18.1 us (3%)
  local copies, waits for them, and re-layouts  15.5 us (2%)
  between operations  13.6 us (2%)
    all_to_all x1, waiting for transfers between devices, per_device(): lax.all_to_all(result, 'ep', split_axis=0, concat_axis=0, tiled=True)  275 us
    all_to_all x1, waiting for transfers between devices, per_device(): lax.all_to_all(outgoing, 'ep', split_axis=0, concat_axis=0, tiled=True)  233 us
    all_gather x1, waiting for transfers between devices, in_one_piece(): lax.all_gather(both, axis, axis=dim, tiled=True)  36.7 us
    all_to_all x1, starting transfers between devices, per_device(): lax.all_to_all(outgoing, 'ep', split_axis=0, concat_axis=0, tiled=True)  32.7 us
    all_to_all x1, starting transfers between devices, per_device(): lax.all_to_all(result, 'ep', split_axis=0, concat_axis=0, tiled=True)  17.5 us
  transfers between devices with their start and end apart: 4, of which 3 were waited for; matrix products, arithmetic and copies ran while one was open for 2% of the time, Pallas kernels for 0%

commit v1 on v0

v1 whole, which is shorter than its diff:
```python
import functools

import jax
import jax.numpy as jnp
from jax import lax
from jax.experimental import pallas as pl
from jax.experimental.pallas import tpu as pltpu
from jax.sharding import PartitionSpec as P

MESH = pl.DeviceIdType.MESH
CHUNK = 64
GROUP = 4


def prefix_sizes(tok, slots, ring):
    far = ring // 2
    sizes = [0] * (far + 2)
    for d in range(1, far + 1):
        rows = min(tok, slots * (far - d) + slots // 2)
        sizes[d] = -(-rows // 16) * 16
    return sizes


def chunks_of(rows):
    return [(lo, min(CHUNK, rows - lo)) for lo in range(0, rows, CHUNK)]


def moe_kernel(
    ring, slots, sizes, offs, shared,
    s_ref, meta_ref, ometa_ref, normed_ref, back_ref, wg_hbm, wu_hbm, wd_hbm,
    out_ref,
    held, meta_held, coming, final, contrib, x_ref, h_ref, o_ref, wj_ref,
    wg, wu, wd,
    d_send, d_recv, m_send, m_recv, r_send, r_recv, w_local, w_send, w_recv,
):
    z = lax.axis_index("ep")
    core = lax.axis_index("tp")
    far = ring // 2
    up = lax.rem(z + 1, ring)
    down = lax.rem(z + ring - 1, ring)
    onward = (up, down)
    home = (down, up)
    tok = s_ref.shape[1]
    pair = 2 * slots

    barrier = pltpu.get_barrier_semaphore()
    pl.semaphore_signal(barrier, inc=1, device_id={"ep": up}, device_id_type=MESH)
    pl.semaphore_signal(barrier, inc=1, device_id={"ep": down}, device_id_type=MESH)
    pl.semaphore_signal(barrier, inc=1, device_id={"tp": 1 - core}, device_id_type=MESH)
    pl.semaphore_wait(barrier, 3)

    def rows_out(way, d, lo, n):
        if d == 0:
            return s_ref.at[way, pl.ds(lo, n)]
        return held.at[way, pl.ds(offs[d] + lo, n)]

    def ring_copy(way, d, i, lo, n):
        return pltpu.make_async_remote_copy(
            src_ref=rows_out(way, d, lo, n),
            dst_ref=held.at[way, pl.ds(offs[d + 1] + lo, n)],
            send_sem=d_send.at[way, d],
            recv_sem=d_recv.at[way, d, i],
            device_id={"ep": onward[way]},
            device_id_type=MESH,
        )

    def meta_copy(way, d):
        return pltpu.make_async_remote_copy(
            src_ref=meta_ref.at[way] if d == 0 else meta_held.at[way, d - 1],
            dst_ref=meta_held.at[way, d],
            send_sem=m_send.at[way, d],
            recv_sem=m_recv.at[way, d],
            device_id={"ep": onward[way]},
            device_id_type=MESH,
        )

    def inbox(way, d, lo, n):
        if d == 0:
            return final.at[way, pl.ds(lo, n)]
        if d <= shared:
            return held.at[way, pl.ds(offs[d] + lo, n)]
        return coming.at[way, pl.ds(offs[d] - offs[shared + 1] + lo, n)]

    def home_copy(way, d, i, lo, n):
        return pltpu.make_async_remote_copy(
            src_ref=inbox(way, d, lo, n),
            dst_ref=inbox(way, d - 1, lo, n),
            send_sem=r_send.at[way, d - 1],
            recv_sem=r_recv.at[way, d - 1, i],
            device_id={"ep": home[way]},
            device_id_type=MESH,
        )

    def send_on(way, d):
        meta_copy(way, d).start()

    for way in (0, 1):
        meta_copy(way, 0).start()
    for i, (lo, n) in enumerate(chunks_of(sizes[1])):
        for way in (0, 1):
            ring_copy(way, 0, i, lo, n).start()

    weights = ((wg_hbm, wg), (wu_hbm, wu), (wd_hbm, wd))

    def own_weight(j):
        src, dst = weights[j]
        return pltpu.make_async_copy(src.at[0], dst.at[0], w_local.at[j])

    def peer_weight(j):
        src, dst = weights[j]
        return pltpu.make_async_remote_copy(
            src_ref=src.at[0], dst_ref=dst.at[1],
            send_sem=w_send.at[j], recv_sem=w_recv.at[j],
            device_id={"tp": 1 - core}, device_id_type=MESH,
        )

    for j in range(3):
        own_weight(j).start()
        peer_weight(j).start()

    slot_row = lax.broadcasted_iota(jnp.int32, (pair, 1), 0)
    base = (z * slots).astype(jnp.float32)
    first = jnp.where(slot_row < slots, base + slot_row.astype(jnp.float32), -2.0)
    second = jnp.where(slot_row >= slots, base + (slot_row - slots).astype(jnp.float32), -2.0)

    def matches(table, wanted):
        a = jnp.where(table[0:1, :] == wanted, 1.0, 0.0)
        b = jnp.where(table[1:2, :] == wanted, 1.0, 0.0)
        return a, b

    def picks(way, d):
        wanted = first if (way == 0 or d == far) else second
        return matches(meta_held[way, d - 1], wanted)

    def own_picks():
        return matches(ometa_ref[...], second)

    def weight_of(table, a, b):
        return jnp.sum(a * table[2:3, :] + b * table[3:4, :], axis=1, keepdims=True)

    def select(d):
        at = ((d - 1) % GROUP) * pair
        rows = sizes[d]
        total = jnp.zeros((pair, s_ref.shape[2]), jnp.float32)
        scale = jnp.zeros((pair, 1), jnp.float32)
        for way in (0, 1):
            a, b = picks(way, d)
            scale = scale + weight_of(meta_held[way, d - 1], a, b)
            one = (a + b).astype(jnp.bfloat16)[:, :rows]
            total = total + jnp.dot(
                one, held[way, pl.ds(offs[d], rows)], preferred_element_type=jnp.float32
            )
        if d == far:
            a, b = own_picks()
            scale = scale + weight_of(ometa_ref[...], a, b)
            total = total + jnp.dot(
                (a + b).astype(jnp.bfloat16), normed_ref[...], preferred_element_type=jnp.float32
            )
        x_ref[pl.ds(at, pair), :] = total.astype(jnp.bfloat16)
        wj_ref[pl.ds(at, pair), :] = jnp.broadcast_to(scale, (pair, wj_ref.shape[1]))

    def ffn(last):
        start = (last - GROUP) * pair
        rows = GROUP * pair
        half = wg.shape[2]
        tile = min(256, half)
        width = x_ref.shape[1]

        @pl.loop(0, 2)
        def _(part):
            for lo in range(0, half, tile):
                g = jnp.dot(x_ref[...], wg[part, :, lo:lo + tile], preferred_element_type=jnp.float32)
                u = jnp.dot(x_ref[...], wu[part, :, lo:lo + tile], preferred_element_type=jnp.float32)
                h_ref[part, :, lo:lo + tile] = ((g / (1.0 + jnp.exp(-g))) * u).astype(jnp.bfloat16)

        cols = min(512, width)

        @pl.loop(0, width // cols)
        def _(c):
            at = pl.ds(pl.multiple_of(c * cols, cols), cols)
            o = jnp.dot(h_ref[0], wd[0, :, at], preferred_element_type=jnp.float32)
            o = o + jnp.dot(h_ref[1], wd[1, :, at], preferred_element_type=jnp.float32)
            o_ref[pl.ds(start, rows), at] = (o * wj_ref[:, 0:1]).astype(jnp.bfloat16)

    for d in range(1, far + 1):
        if d >= 3:
            for way in (0, 1):
                ring_copy(way, d - 3, 0, 0, sizes[d - 2]).wait_send()
                meta_copy(way, d - 3).wait_send()
        for way in (0, 1):
            meta_copy(way, d - 1).wait_recv()
            if d < far:
                meta_copy(way, d).start()
        onwards = dict((lo, n) for lo, n in chunks_of(sizes[d + 1])) if d < far else {}
        for i, (lo, n) in enumerate(chunks_of(sizes[d])):
            for way in (0, 1):
                ring_copy(way, d - 1, i, lo, n).wait_recv()
                if lo in onwards:
                    ring_copy(way, d, i, lo, onwards[lo]).start()
        if d == GROUP:
            for j in range(3):
                own_weight(j).wait()
                peer_weight(j).wait()
        select(d)
        if d % GROUP == 0:
            ffn(d)
    for d in (far - 2, far - 1):
        for way in (0, 1):
            ring_copy(way, d, 0, 0, sizes[d + 1]).wait_send()
            meta_copy(way, d).wait_send()

    def contributions(way, d):
        a, b = picks(way, d)
        one = (a + b).astype(jnp.bfloat16)[:, :sizes[d]]
        got = lax.dot_general(
            one, o_ref[pl.ds((d - 1) * pair, pair), :], (((0,), (0,)), ((), ())),
            preferred_element_type=jnp.float32,
        )
        contrib[way, pl.ds(0, sizes[d])] = got.astype(jnp.bfloat16)

    for d in range(far, 0, -1):
        for way in (0, 1):
            contributions(way, d)
        arriving = dict((lo, n) for lo, n in chunks_of(sizes[d + 1])) if d < far else {}
        for i, (lo, n) in enumerate(chunks_of(sizes[d])):
            for way in (0, 1):
                m = arriving.get(lo, 0)
                if m:
                    home_copy(way, d + 1, i, lo, m).wait_recv()
                    was = inbox(way, d, lo, m)
                    was[...] = (
                        was[...].astype(jnp.float32)
                        + contrib[way, pl.ds(lo, m)].astype(jnp.float32)
                    ).astype(jnp.bfloat16)
                if m < n:
                    inbox(way, d, lo + m, n - m)[...] = contrib[way, pl.ds(lo + m, n - m)]
                home_copy(way, d, i, lo, n).start()
    for i, (lo, n) in enumerate(chunks_of(sizes[1])):
        for way in (0, 1):
            home_copy(way, 1, i, lo, n).wait_recv()

    a, b = own_picks()
    own = (a + b).astype(jnp.bfloat16)
    width = out_ref.shape[1]
    cols = min(512, width)

    @pl.loop(0, width // cols)
    def _(c):
        at = pl.ds(pl.multiple_of(c * cols, cols), cols)
        got = jnp.dot(back_ref[0], final[0, :, at], preferred_element_type=jnp.float32)
        got = got + jnp.dot(back_ref[1], final[1, :, at], preferred_element_type=jnp.float32)
        got = got + lax.dot_general(
            own, o_ref[pl.ds((far - 1) * pair, pair), at], (((0,), (0,)), ((), ())),
            preferred_element_type=jnp.float32,
        )
        out_ref[:, at] = got.astype(out_ref.dtype)

    for d in range(far, 0, -1):
        for way in (0, 1):
            home_copy(way, d, 0, 0, sizes[d]).wait_send()


def per_device(tokens, norm_gain, expert_ids, route_weights, w_gate, w_up, w_down):
    tok, width = tokens.shape
    top = expert_ids.shape[1]
    ring = lax.axis_size("ep")
    experts = w_gate.shape[0] * ring
    slots = 3 * tok * top // (2 * experts)
    far = ring // 2
    sizes = prefix_sizes(tok, slots, ring)
    offs, at = ([0] * (far + 2), 0)
    for d in range(1, far + 2):
        offs[d] = at
        at += sizes[d]
    total = at
    shared = far - 4
    half = w_gate.shape[2]
    pair = 2 * slots

    z = lax.axis_index("ep")
    values = tokens.astype(jnp.float32)
    scale = lax.rsqrt(jnp.mean(values * values, axis=-1, keepdims=True) + 1e-06)
    normed = (values * scale * norm_gain).astype(jnp.bfloat16)

    flat = expert_ids.reshape(-1)
    onehot = (flat[:, None] == jnp.arange(experts, dtype=jnp.int32)[None, :]).astype(jnp.bfloat16)
    count = tok * top
    earlier = (jnp.arange(count)[:, None] > jnp.arange(count)[None, :]).astype(jnp.bfloat16)
    before = jnp.dot(earlier, onehot, preferred_element_type=jnp.float32)
    slot = jnp.sum(before * onehot.astype(jnp.float32), axis=1).astype(jnp.int32).reshape(tok, top)
    target = (expert_ids * slots + slot).astype(jnp.float32)
    off = lax.rem(expert_ids - z + ring, ring)
    plus = ((off >= 1) & (off < far)) | ((off == far) & (slot < slots // 2))
    minus = (off > 0) & ~plus
    tables, backs, sorted_rows = ([], [], [])
    for mask, dist in ((plus, off), (minus, ring - off)):
        reach = jnp.max(jnp.where(mask, dist, 0), axis=1)
        ahead = (reach[None, :] > reach[:, None]) | (
            (reach[None, :] == reach[:, None])
            & (jnp.arange(tok)[None, :] < jnp.arange(tok)[:, None])
        )
        place = jnp.sum(ahead.astype(jnp.int32), axis=1)
        back = (place[:, None] == jnp.arange(tok)[None, :])
        table = jnp.concatenate(
            [jnp.where(mask, target, -1.0).T, route_weights.T, jnp.zeros((4, tok), jnp.float32)]
        )
        tables.append(jnp.dot(table, back.astype(jnp.float32), precision=lax.Precision.HIGHEST))
        back = back.astype(jnp.bfloat16)
        backs.append(back)
        sorted_rows.append(
            lax.dot_general(
                back, normed, (((0,), (0,)), ((), ())), preferred_element_type=jnp.float32
            ).astype(jnp.bfloat16)
        )
    own_table = jnp.concatenate(
        [jnp.where(off == 0, target, -1.0).T, route_weights.T, jnp.zeros((4, tok), jnp.float32)]
    )

    vm = pl.BlockSpec(memory_space=pltpu.VMEM)
    hbm = pl.BlockSpec(memory_space=pl.ANY)
    most = len(chunks_of(tok))
    bf16, f32 = jnp.bfloat16, jnp.float32
    call = pl.pallas_call(
        functools.partial(moe_kernel, ring, slots, sizes, offs, shared),
        out_shape=jax.ShapeDtypeStruct((tok, width), bf16),
        in_specs=[vm, vm, vm, vm, vm, hbm, hbm, hbm],
        out_specs=vm,
        scratch_shapes=[
            pltpu.VMEM((2, total, width), bf16),
            pltpu.VMEM((2, far, 8, tok), f32),
            pltpu.VMEM((2, total - offs[shared + 1], width), bf16),
            pltpu.VMEM((2, tok, width), bf16),
            pltpu.VMEM((2, tok, width), bf16),
            pltpu.VMEM((GROUP * pair, width), bf16),
            pltpu.VMEM((2, GROUP * pair, half), bf16),
            pltpu.VMEM((far * pair, width), bf16),
            pltpu.VMEM((GROUP * pair, 128), f32),
            pltpu.VMEM((2, width, half), bf16),
            pltpu.VMEM((2, width, half), bf16),
            pltpu.VMEM((2, half, width), bf16),
            pltpu.SemaphoreType.DMA((2, far)),
            pltpu.SemaphoreType.DMA((2, far, most)),
            pltpu.SemaphoreType.DMA((2, far)),
            pltpu.SemaphoreType.DMA((2, far)),
            pltpu.SemaphoreType.DMA((2, far)),
            pltpu.SemaphoreType.DMA((2, far, most)),
            pltpu.SemaphoreType.DMA((3,)),
            pltpu.SemaphoreType.DMA((3,)),
            pltpu.SemaphoreType.DMA((3,)),
        ],
        compiler_params=pltpu.CompilerParams(
            collective_id=0, has_side_effects=True, vmem_limit_bytes=67043328
        ),
        cost_estimate=pl.CostEstimate(
            flops=12 * tok * top * width * half, bytes_accessed=24 * width * half, transcendentals=0
        ),
    )
    return call(
        jnp.stack(sorted_rows), jnp.stack(tables), own_table, normed, jnp.stack(backs),
        w_gate, w_up, w_down,
    )


def solution(mesh):
    in_specs = (
        P(("grp", "ep", "tp"), None),
        P(),
        P(("grp", "ep", "tp"), None),
        P(("grp", "ep", "tp"), None),
        P("ep", None, "tp"),
        P("ep", None, "tp"),
        P("ep", "tp", None),
    )
    out_specs = P(("grp", "ep", "tp"), None)
    return jax.shard_map(
        per_device, mesh=mesh, in_specs=in_specs, out_specs=out_specs, check_vma=False
    )
```

time: 671 us -> 558 us (0.83)
  waiting for transfers between devices: 546 us -> 0 us
  Pallas kernels: 0 us -> 543 us
  starting transfers between devices: 50.3 us -> 0 us
  matrix products: 18.1 us -> 1.86 us
  other arithmetic: 22.2 us -> 8.03 us
  between operations: 13.6 us -> 0.12 us
  local copies, waits for them, and re-layouts: 15.5 us -> 4.06 us
    pallas_call x0 -> x1, Pallas kernels: none -> 543 us  [per_device(): call(jnp.stack(sorted_rows), jnp.stack(tables), own_table, normed, jnp.st...]
    all_to_all x2 -> x0, waiting for transfers between devices: 508 us -> none  [the longest x1 275 us: per_device(): lax.all_to_all(result, 'ep', split_axis=0, concat_axis=0, tiled=True)]
    all_to_all x2 -> x0, starting transfers between devices: 50.1 us -> none  [the longest x1 32.7 us: per_device(): lax.all_to_all(outgoing, 'ep', split_axis=0, concat_axis=0, tiled=True)]
    all_gather x2 -> x0, waiting for transfers between devices: 36.7 us -> none  [the longest x1 36.7 us: in_one_piece(): lax.all_gather(both, axis, axis=dim, tiled=True)]
    dot_general x3 -> x5, matrix products: 18.1 us -> 1.86 us  [the longest x2 1.11 us: per_device(): lax.dot_general(back, normed, (((0,), (0,)), ((), ())), preferred_element...]
    gather x3 -> x0, local copies, waits for them, and re-layouts: 10.8 us -> none  [the longest x2 6.5 us: per_device(): jnp.take(results, target, axis=0).reshape(tok_rows, top_count, width)]
    reduce_sum x2 -> x1, other arithmetic: 9.31 us -> 0.27 us  [per_device(): place = jnp.sum(ahead.astype(jnp.int32), axis=1)]
  transfers between devices with their start and end apart: 4 -> 0, of which waited for: 3 -> 0; matrix products, arithmetic and copies ran while one was open for 2% -> 0% of each run, Pallas kernels for 0% -> 0%
where the time goes in v1:
time: 558 us; the launch traced here: 557 us
  Pallas kernels  543 us (97%)
  other arithmetic  8.03 us (1%)
    pallas_call x1, Pallas kernels, per_device(): call(jnp.stack(sorted_rows), jnp.stack(tables), own_table, normed, jnp.st...  543 us

profile of v1, /device:TPU:46, one launch (start us, length us, event | category | flops | bytes accessed | tf_op | source)
XLA Modules:
  0.0 557.2 jit_solution(8409790983234706349)
XLA Ops:
  0.0 0.0 copy-start.1
  0.0 0.9 copy.11
  0.9 0.1 eq.84
  1.1 0.3 fusion.5
  1.3 0.1 convert_element_type.56
  1.5 0.1 copy.12
  1.6 0.7 fusion.25
  2.3 0.7 select_bitcast_fusion.1
  3.0 0.3 convert_reduce_fusion
  3.3 1.5 fusion.2
  4.8 0.0 copy-done.1
  4.8 1.0 fusion.4.normed_ref
  5.8 0.0 copy-start
  5.8 0.6 fusion
  6.4 0.4 copy-done
  6.8 0.6 fusion.1
  7.3 0.0 copy-start.2
  7.3 0.0 copy-start.3
  7.4 1.5 pad_maximum_fusion.s_ref
  8.9 0.0 copy-done.2
  8.9 0.1 pad.12.clone
  9.0 0.0 copy-done.3
  9.0 0.2 convolution_bitcast_fusion
  9.2 0.3 convolution_bitcast_fusion.1
  9.5 0.7 pad_maximum_fusion.1.meta_ref
  10.1 0.1 iota_compare_fusion.2
  10.2 0.1 iota_compare_fusion.3
  10.3 0.7 add_convert_fusion.back_ref
  11.1 0.7 fusion.20.ometa_ref
  11.8 543.1 %shard_map.73 = bf16[256,2048]{1,0:T(8,128)(2,1)} custom-call(bf16[2,256,2048]{2,1,0:T(8,128)(2,1)} %pad_maximum_fusion.s_ref, f32[2,8,256]{2,1,0:T(8,128)} %pad_maximum_fusion.1.meta_ref, f32[8,256]{1,0:T(8,128)} %fusion.20.ometa_ref, bf16[256,2048]{1,0:T(8,128)(2,1)} %copy-done, bf16[2,256,256]{2,1,0:T(8,128)(2,1)} %add_convert_fusion.back_ref, ...), custom_call_target="tpu_custom_call" | custom-call | flops 6442450944 | bytes 25165824 | tf_op jit(solution)/shard_map/pallas_call | solution.py:358
  554.9 2.3 copy.15
  (5 shorter events, 0.0 us)
Async XLA Ops:
  0.0 4.8 copy-start.1
  5.8 1.0 copy-start
  7.3 1.6 copy-start.2
  7.3 1.6 copy-start.3

commit v2 on v1

v2 whole, which is shorter than its diff:
```python
import functools

import jax
import jax.numpy as jnp
from jax import lax
from jax.experimental import pallas as pl
from jax.experimental.pallas import tpu as pltpu
from jax.sharding import PartitionSpec as P

MESH = pl.DeviceIdType.MESH
CHUNK = 64
REACH = 5


def prefix_sizes(tok, slots, far, reach):
    last = far - reach
    near = reach // 2
    sizes = [0] * (last + 2)
    for d in range(1, last + 1):
        rows = slots * (last - d) + slots // 2 + 2 * slots * max(0, near - d + 1)
        sizes[d] = -(-min(tok, rows) // 16) * 16
    return sizes


def chunks_of(rows):
    return [(lo, min(CHUNK, rows - lo)) for lo in range(0, rows, CHUNK)]


def block_plan(far, reach):
    near = reach // 2
    order = {0: [], 1: [], 2: []}
    for d in range(0, far - reach + 1):
        ways = (0,) if d == 0 else (0, 1)
        for way in ways:
            for copy in (0, 1, 2):
                main = d == 0 or copy == 1 + way
                if main or d <= near:
                    order[copy].append((way, d))
    places, at = ({}, 0)
    spans = {}
    for copy in (0, 1, 2):
        spans[copy] = at
        for key in order[copy]:
            places[(copy,) + key] = at
            at += 1
    return order, places, spans, at


def moe_kernel(
    ring, groups, slots, sizes, offs, shared,
    s_ref, meta_ref, sorted_own_ref, own_ref, back_ref, wg_hbm, wu_hbm, wd_hbm,
    out_ref,
    held, meta_held, coming, final, contrib, x_ref, h_ref, wj_ref,
    wg, wu, wd,
    d_send, d_recv, m_send, m_recv, r_send, r_recv,
    own_local, pair_send, pair_recv, far_send, far_recv, side_send, side_recv,
):
    g = lax.axis_index("grp")
    z = lax.axis_index("ep")
    core = lax.axis_index("tp")
    far = ring // 2
    last = far - REACH
    near = REACH // 2
    up = lax.rem(z + 1, ring)
    down = lax.rem(z + ring - 1, ring)
    far_up = lax.rem(z + REACH, ring)
    far_down = lax.rem(z + ring - REACH, ring)
    onward = (up, down)
    home = (down, up)
    block = -(-slots // 16) * 16
    order, places, spans, _ = block_plan(far, REACH)

    barrier = pltpu.get_barrier_semaphore()
    for there in (up, down, far_up, far_down):
        pl.semaphore_signal(barrier, inc=1, device_id={"ep": there}, device_id_type=MESH)
    pl.semaphore_signal(barrier, inc=1, device_id={"tp": 1 - core}, device_id_type=MESH)

    @pl.loop(1, groups)
    def _(j):
        pl.semaphore_signal(
            barrier, inc=1, device_id={"grp": lax.rem(g + j, groups)}, device_id_type=MESH
        )

    pl.semaphore_wait(barrier, 4 + groups)

    weights = ((wg_hbm, wg), (wu_hbm, wu), (wd_hbm, wd))

    def shard(j, which):
        rows = weights[j][0].shape[1] // groups
        return pl.ds(pl.multiple_of(which * rows, rows), rows)

    def far_copy(j, copy):
        src, dst = weights[j]
        return pltpu.make_async_remote_copy(
            src_ref=src.at[0, shard(j, g)],
            dst_ref=dst.at[copy, 0, shard(j, g)],
            send_sem=far_send.at[copy - 1, j],
            recv_sem=far_recv.at[copy - 1, j],
            device_id={"ep": far_down if copy == 1 else far_up},
            device_id_type=MESH,
        )

    def side_copy(j, copy, step, whose):
        ref = weights[j][1].at[copy, 0, shard(j, whose)]
        return pltpu.make_async_remote_copy(
            src_ref=ref, dst_ref=ref,
            send_sem=side_send.at[copy - 1, j, step],
            recv_sem=side_recv.at[copy - 1, j, step],
            device_id={"grp": lax.rem(g + step, groups)},
            device_id_type=MESH,
        )

    def pair_copy(j, copy):
        src, dst = weights[j]
        return pltpu.make_async_remote_copy(
            src_ref=src.at[0] if copy == 0 else dst.at[copy, 0],
            dst_ref=dst.at[copy, 1],
            send_sem=pair_send.at[copy, j],
            recv_sem=pair_recv.at[copy, j],
            device_id={"tp": 1 - core},
            device_id_type=MESH,
        )

    def own_weight(j):
        src, dst = weights[j]
        return pltpu.make_async_copy(src.at[0], dst.at[0, 0], own_local.at[j])

    def rows_out(way, d, lo, n):
        if d == 0:
            return s_ref.at[way, pl.ds(lo, n)]
        return held.at[way, pl.ds(offs[d] + lo, n)]

    def ring_copy(way, d, i, lo, n):
        return pltpu.make_async_remote_copy(
            src_ref=rows_out(way, d, lo, n),
            dst_ref=held.at[way, pl.ds(offs[d + 1] + lo, n)],
            send_sem=d_send.at[way, d],
            recv_sem=d_recv.at[way, d, i],
            device_id={"ep": onward[way]},
            device_id_type=MESH,
        )

    def meta_copy(way, d):
        return pltpu.make_async_remote_copy(
            src_ref=meta_ref.at[way] if d == 0 else meta_held.at[way, d - 1],
            dst_ref=meta_held.at[way, d],
            send_sem=m_send.at[way, d],
            recv_sem=m_recv.at[way, d],
            device_id={"ep": onward[way]},
            device_id_type=MESH,
        )

    def inbox(way, d, lo, n):
        if d == 0:
            return final.at[way, pl.ds(lo, n)]
        if d <= shared:
            return held.at[way, pl.ds(offs[d] + lo, n)]
        return coming.at[way, pl.ds(offs[d] - offs[shared + 1] + lo, n)]

    def home_copy(way, d, i, lo, n):
        return pltpu.make_async_remote_copy(
            src_ref=inbox(way, d, lo, n),
            dst_ref=inbox(way, d - 1, lo, n),
            send_sem=r_send.at[way, d - 1],
            recv_sem=r_recv.at[way, d - 1, i],
            device_id={"ep": home[way]},
            device_id_type=MESH,
        )

    for way in (0, 1):
        meta_copy(way, 0).start()
    for j in range(3):
        for copy in (1, 2):
            far_copy(j, copy).start()
    for i, (lo, n) in enumerate(chunks_of(sizes[1])):
        for way in (0, 1):
            ring_copy(way, 0, i, lo, n).start()
    for j in range(3):
        own_weight(j).start()
        pair_copy(j, 0).start()

    slot_row = lax.broadcasted_iota(jnp.int32, (block, 1), 0).astype(jnp.float32)
    wanted = tuple(
        jnp.where(slot_row < slots, (expert * slots).astype(jnp.float32) + slot_row, -2.0)
        for expert in (z, far_up, far_down)
    )

    def matches(table, copy):
        a = jnp.where(table[0:1, :] == wanted[copy], 1.0, 0.0)
        b = jnp.where(table[1:2, :] == wanted[copy], 1.0, 0.0)
        return a, b

    def table_of(way, d):
        return sorted_own_ref[...] if d == 0 else meta_held[way, d - 1]

    def select(way, d):
        rows = s_ref.shape[1] if d == 0 else sizes[d]
        table = table_of(way, d)
        for copy in (0, 1, 2):
            if (copy, way, d) not in places:
                continue
            at = pl.ds(places[(copy, way, d)] * block, block)
            a, b = matches(table, copy)
            scale = jnp.sum(a * table[2:3, :] + b * table[3:4, :], axis=1, keepdims=True)
            one = (a + b).astype(jnp.bfloat16)[:, :rows]
            source = s_ref[0] if d == 0 else held[way, pl.ds(offs[d], rows)]
            got = jnp.dot(one, source, preferred_element_type=jnp.float32)
            x_ref[at, :] = got.astype(jnp.bfloat16)
            wj_ref[at, :] = jnp.broadcast_to(scale, (block, wj_ref.shape[1]))

    def ffn(copy, lo_block, hi_block):
        start = (spans[copy] + lo_block) * block
        rows = (hi_block - lo_block) * block
        here = pl.ds(start, rows)
        half = wg.shape[3]
        tile = min(256, half)
        width = x_ref.shape[1]

        @pl.loop(0, 2)
        def _(part):
            for lo in range(0, half, tile):
                x = x_ref[here, :]
                a = jnp.dot(x, wg[copy, part, :, lo:lo + tile], preferred_element_type=jnp.float32)
                u = jnp.dot(x, wu[copy, part, :, lo:lo + tile], preferred_element_type=jnp.float32)
                h_ref[part, pl.ds(0, rows), lo:lo + tile] = (
                    (a / (1.0 + jnp.exp(-a))) * u
                ).astype(jnp.bfloat16)

        cols = min(512, width)

        @pl.loop(0, width // cols)
        def _(c):
            at = pl.ds(pl.multiple_of(c * cols, cols), cols)
            o = jnp.dot(h_ref[0, pl.ds(0, rows), :], wd[copy, 0, :, at], preferred_element_type=jnp.float32)
            o = o + jnp.dot(h_ref[1, pl.ds(0, rows), :], wd[copy, 1, :, at], preferred_element_type=jnp.float32)
            x_ref[here, at] = (o * wj_ref[here, 0:1]).astype(jnp.bfloat16)

    def upto(copy, d):
        return len([1 for key in order[copy] if key[1] <= d])

    def spread_weights():
        for j in range(3):
            for copy in (1, 2):
                far_copy(j, copy).wait_recv()

                @pl.loop(1, groups)
                def _(step):
                    side_copy(j, copy, step, g).start()

    def pair_weights():
        for j in range(3):
            for copy in (1, 2):

                @pl.loop(1, groups)
                def _(step):
                    side_copy(j, copy, step, lax.rem(g + groups - step, groups)).wait_recv()

                pair_copy(j, copy).start()

    def finish_weights():
        for j in range(3):
            for copy in (1, 2):
                pair_copy(j, copy).wait()
                far_copy(j, copy).wait_send()

                @pl.loop(1, groups)
                def _(step):
                    side_copy(j, copy, step, g).wait_send()

    select(0, 0)
    mid = (last + near + 1) // 2
    spread_weights()
    for d in range(1, last + 1):
        if d >= 3:
            for way in (0, 1):
                ring_copy(way, d - 3, 0, 0, sizes[d - 2]).wait_send()
                meta_copy(way, d - 3).wait_send()
        for way in (0, 1):
            meta_copy(way, d - 1).wait_recv()
            if d < last:
                meta_copy(way, d).start()
        onwards = dict((lo, n) for lo, n in chunks_of(sizes[d + 1])) if d < last else {}
        for i, (lo, n) in enumerate(chunks_of(sizes[d])):
            for way in (0, 1):
                ring_copy(way, d - 1, i, lo, n).wait_recv()
                if lo in onwards:
                    ring_copy(way, d, i, lo, onwards[lo]).start()
        for way in (0, 1):
            select(way, d)
        if d == near:
            for j in range(3):
                own_weight(j).wait()
                pair_copy(j, 0).wait()
            ffn(0, 0, upto(0, near))
            pair_weights()
        if d == mid:
            finish_weights()
            ffn(1, 0, upto(1, mid))
        if d == mid + 1:
            ffn(2, 0, upto(2, mid + 1))
    ffn(1, upto(1, mid), upto(1, last))
    ffn(2, upto(2, mid + 1), upto(2, last))
    for d in (last - 2, last - 1):
        for way in (0, 1):
            ring_copy(way, d, 0, 0, sizes[d + 1]).wait_send()
            meta_copy(way, d).wait_send()

    def gathered(table, rows, way, d, at):
        got = None
        for copy in (0, 1, 2):
            if (copy, way, d) not in places:
                continue
            a, b = matches(table, copy)
            one = (a + b).astype(jnp.bfloat16)[:, :rows]
            part = lax.dot_general(
                one, x_ref[pl.ds(places[(copy, way, d)] * block, block), at],
                (((0,), (0,)), ((), ())), preferred_element_type=jnp.float32,
            )
            got = part if got is None else got + part
        return got

    for d in range(last, 0, -1):
        for way in (0, 1):
            got = gathered(meta_held[way, d - 1], sizes[d], way, d, slice(None))
            contrib[way, pl.ds(0, sizes[d])] = got.astype(jnp.bfloat16)
        arriving = dict((lo, n) for lo, n in chunks_of(sizes[d + 1])) if d < last else {}
        for i, (lo, n) in enumerate(chunks_of(sizes[d])):
            for way in (0, 1):
                m = arriving.get(lo, 0)
                if m:
                    home_copy(way, d + 1, i, lo, m).wait_recv()
                    was = inbox(way, d, lo, m)
                    was[...] = (
                        was[...].astype(jnp.float32)
                        + contrib[way, pl.ds(lo, m)].astype(jnp.float32)
                    ).astype(jnp.bfloat16)
                if m < n:
                    inbox(way, d, lo + m, n - m)[...] = contrib[way, pl.ds(lo + m, n - m)]
                home_copy(way, d, i, lo, n).start()
    for i, (lo, n) in enumerate(chunks_of(sizes[1])):
        for way in (0, 1):
            home_copy(way, 1, i, lo, n).wait_recv()

    tok, width = out_ref.shape
    cols = min(512, width)

    @pl.loop(0, width // cols)
    def _(c):
        at = pl.ds(pl.multiple_of(c * cols, cols), cols)
        got = jnp.dot(back_ref[0], final[0, :, at], preferred_element_type=jnp.float32)
        got = got + jnp.dot(back_ref[1], final[1, :, at], preferred_element_type=jnp.float32)
        got = got + gathered(own_ref[...], tok, 0, 0, at)
        out_ref[:, at] = got.astype(out_ref.dtype)

    for d in range(last, 0, -1):
        for way in (0, 1):
            home_copy(way, d, 0, 0, sizes[d]).wait_send()


def per_device(tokens, norm_gain, expert_ids, route_weights, w_gate, w_up, w_down):
    tok, width = tokens.shape
    top = expert_ids.shape[1]
    ring = lax.axis_size("ep")
    groups = lax.axis_size("grp")
    experts = w_gate.shape[0] * ring
    slots = 3 * tok * top // (2 * experts)
    far = ring // 2
    last = far - REACH
    near = REACH // 2
    sizes = prefix_sizes(tok, slots, far, REACH)
    offs, at = ([0] * (last + 2), 0)
    for d in range(1, last + 2):
        offs[d] = at
        at += sizes[d]
    total = at
    shared = last - 4
    half = w_gate.shape[2]
    block = -(-slots // 16) * 16
    order, places, spans, blocks = block_plan(far, REACH)
    mid = (last + near + 1) // 2
    widest = max(
        len([1 for key in order[1] if key[1] <= mid]), len([1 for key in order[2] if key[1] <= mid + 1])
    )

    z = lax.axis_index("ep")
    values = tokens.astype(jnp.float32)
    scale = lax.rsqrt(jnp.mean(values * values, axis=-1, keepdims=True) + 1e-06)
    normed = (values * scale * norm_gain).astype(jnp.bfloat16)

    flat = expert_ids.reshape(-1)
    onehot = (flat[:, None] == jnp.arange(experts, dtype=jnp.int32)[None, :]).astype(jnp.bfloat16)
    count = tok * top
    earlier = (jnp.arange(count)[:, None] > jnp.arange(count)[None, :]).astype(jnp.bfloat16)
    before = jnp.dot(earlier, onehot, preferred_element_type=jnp.float32)
    slot = jnp.sum(before * onehot.astype(jnp.float32), axis=1).astype(jnp.int32).reshape(tok, top)
    target = (expert_ids * slots + slot).astype(jnp.float32)
    off = lax.rem(expert_ids - z + ring, ring)
    ahead_half = (off < far) | ((off == far) & (slot < slots // 2))
    signed = jnp.where(ahead_half, off, off - ring)
    host = jnp.where(
        jnp.abs(signed) <= near, signed, jnp.where(signed > 0, signed - REACH, signed + REACH)
    )
    extra = [route_weights.T, jnp.zeros((4, tok), jnp.float32)]
    own_table = jnp.concatenate([jnp.where(host == 0, target, -1.0).T] + extra)
    tables, backs, sorted_rows = ([], [], [])
    for dist in (host, -host):
        reach = jnp.max(jnp.maximum(dist, 0), axis=1)
        ahead = (reach[None, :] > reach[:, None]) | (
            (reach[None, :] == reach[:, None])
            & (jnp.arange(tok)[None, :] < jnp.arange(tok)[:, None])
        )
        place = jnp.sum(ahead.astype(jnp.int32), axis=1)
        back = (place[:, None] == jnp.arange(tok)[None, :])
        table = jnp.concatenate([jnp.where(dist > 0, target, -1.0).T] + extra)
        if not tables:
            table = jnp.concatenate([table, own_table])
        tables.append(jnp.dot(table, back.astype(jnp.float32), precision=lax.Precision.HIGHEST))
        back = back.astype(jnp.bfloat16)
        backs.append(back)
        sorted_rows.append(
            lax.dot_general(
                back, normed, (((0,), (0,)), ((), ())), preferred_element_type=jnp.float32
            ).astype(jnp.bfloat16)
        )
    sorted_own = tables[0][8:]
    tables[0] = tables[0][:8]

    vm = pl.BlockSpec(memory_space=pltpu.VMEM)
    hbm = pl.BlockSpec(memory_space=pl.ANY)
    most = len(chunks_of(tok))
    bf16, f32 = jnp.bfloat16, jnp.float32
    call = pl.pallas_call(
        functools.partial(moe_kernel, ring, groups, slots, sizes, offs, shared),
        out_shape=jax.ShapeDtypeStruct((tok, width), bf16),
        in_specs=[vm, vm, vm, vm, vm, hbm, hbm, hbm],
        out_specs=vm,
        scratch_shapes=[
            pltpu.VMEM((2, total, width), bf16),
            pltpu.VMEM((2, last, 8, tok), f32),
            pltpu.VMEM((2, total - offs[shared + 1], width), bf16),
            pltpu.VMEM((2, tok, width), bf16),
            pltpu.VMEM((2, tok, width), bf16),
            pltpu.VMEM((blocks * block, width), bf16),
            pltpu.VMEM((2, widest * block, half), bf16),
            pltpu.VMEM((blocks * block, 128), f32),
            pltpu.VMEM((3, 2, width, half), bf16),
            pltpu.VMEM((3, 2, width, half), bf16),
            pltpu.VMEM((3, 2, half, width), bf16),
            pltpu.SemaphoreType.DMA((2, last)),
            pltpu.SemaphoreType.DMA((2, last, most)),
            pltpu.SemaphoreType.DMA((2, last)),
            pltpu.SemaphoreType.DMA((2, last)),
            pltpu.SemaphoreType.DMA((2, last)),
            pltpu.SemaphoreType.DMA((2, last, most)),
            pltpu.SemaphoreType.DMA((3,)),
            pltpu.SemaphoreType.DMA((3, 3)),
            pltpu.SemaphoreType.DMA((3, 3)),
            pltpu.SemaphoreType.DMA((2, 3)),
            pltpu.SemaphoreType.DMA((2, 3)),
            pltpu.SemaphoreType.DMA((2, 3, groups)),
            pltpu.SemaphoreType.DMA((2, 3, groups)),
        ],
        compiler_params=pltpu.CompilerParams(
            collective_id=0, has_side_effects=True, vmem_limit_bytes=67043328
        ),
        cost_estimate=pl.CostEstimate(
            flops=12 * tok * top * width * half, bytes_accessed=24 * width * half, transcendentals=0
        ),
    )
    return call(
        jnp.stack(sorted_rows), jnp.stack(tables), sorted_own, own_table, jnp.stack(backs),
        w_gate, w_up, w_down,
    )


def solution(mesh):
    in_specs = (
        P(("grp", "ep", "tp"), None),
        P(),
        P(("grp", "ep", "tp"), None),
        P(("grp", "ep", "tp"), None),
        P("ep", None, "tp"),
        P("ep", None, "tp"),
        P("ep", "tp", None),
    )
    out_specs = P(("grp", "ep", "tp"), None)
    return jax.shard_map(
        per_device, mesh=mesh, in_specs=in_specs, out_specs=out_specs, check_vma=False
    )
```

time: 558 us -> 511 us (0.916)
  Pallas kernels: 543 us -> 497 us
    pallas_call x1, Pallas kernels: 543 us -> 497 us  [per_device(): call(jnp.stack(sorted_rows), jnp.stack(tables), sorted_own, own_table, jn...]
where the time goes in v2:
time: 511 us
  Pallas kernels  497 us (97%)
  other arithmetic  6.3 us (1%)
    pallas_call x1, Pallas kernels, per_device(): call(jnp.stack(sorted_rows), jnp.stack(tables), sorted_own, own_table, jn...  497 us

profile of v2, /device:TPU:46, one launch (start us, length us, event | category | flops | bytes accessed | tf_op | source)
XLA Modules:
  0.0 510.8 jit_solution(16734774550740659326)
XLA Ops:
  0.0 0.0 copy-start
  0.0 0.0 copy-start.1
  0.0 1.6 fusion.2
  1.6 0.8 copy.11
  2.4 0.1 eq.84
  2.6 0.3 fusion.5
  2.9 0.1 convert_element_type.56
  3.0 0.1 copy.12
  3.1 0.7 fusion.21
  3.8 0.3 convert_reduce_fusion
  4.1 1.8 fusion.1
  5.9 0.0 copy-done
  6.0 0.0 copy-done.1
  6.0 0.6 fusion
  6.6 0.0 copy-start.2
  6.6 0.0 copy-start.3
  6.6 1.5 pad_maximum_fusion.s_ref
  8.1 0.0 copy-done.2
  8.2 0.0 copy-done.3
  8.2 0.2 convolution_bitcast_fusion
  8.4 0.1 concatenate.10
  8.5 0.2 fusion.8
  8.7 0.6 fusion.25
  9.3 0.6 pad_maximum_fusion.1.meta_ref
  9.9 0.6 pad_maximum_fusion.2.own_ref
  10.6 0.1 iota_compare_fusion.2
  10.7 0.1 iota_compare_fusion.3
  10.8 0.7 add_convert_fusion.back_ref
  11.5 496.9 %shard_map.73 = bf16[256,2048]{1,0:T(8,128)(2,1)} custom-call(bf16[2,256,2048]{2,1,0:T(8,128)(2,1)} %pad_maximum_fusion.s_ref, f32[2,8,256]{2,1,0:T(8,128)} %pad_maximum_fusion.1.meta_ref, f32[8,256]{1,0:T(8,128)} %get-tuple-element.9.sorted_own_ref, f32[8,256]{1,0:T(8,128)} %pad_maximum_fusion.2.own_ref, bf16[2,256,256]{2,1,0:T(8,128)(2,1)} %add_convert_fusion.back_ref, ...), custom_call_target="tpu_custom_call" | custom-call | flops 6442450944 | bytes 25165824 | tf_op jit(solution)/shard_map/pallas_call | solution.py:470
  508.5 2.3 copy.15
  (5 shorter events, 0.0 us)
Async XLA Ops:
  0.0 5.9 %copy-start = (bf16[256,2048]{1,0:T(8,128)(2,1)S(1)}, bf16[256,2048]{1,0:T(8,128)(2,1)}, u32[]{:S(2)}) copy-start(bf16[256,2048]{1,0:T(8,128)(2,1)} %param.7) | copy-start | bytes 3145732
  0.0 6.0 %copy-start.1 = (f32[2048]{0:T(1024)S(1)}, f32[2048]{0:T(1024)}, u32[]{:S(2)}) copy-start(f32[2048]{0:T(1024)} %param.8) | copy-start | bytes 24580
  6.6 1.6 copy-start.2
  6.6 1.6 copy-start.3

commit v3 on v2

--- a/solution.py
+++ b/solution.py
@@ -8,7 +8,7 @@
 from jax.sharding import PartitionSpec as P
 
 MESH = pl.DeviceIdType.MESH
-CHUNK = 64
+STEPS = (0, 16, 32, 64, 128, 192)
 REACH = 5
 
 
@@ -18,12 +18,13 @@
     sizes = [0] * (last + 2)
     for d in range(1, last + 1):
         rows = slots * (last - d) + slots // 2 + 2 * slots * max(0, near - d + 1)
-        sizes[d] = -(-min(tok, rows) // 16) * 16
+        sizes[d] = -(-min(tok, rows) // 8) * 8
     return sizes
 
 
 def chunks_of(rows):
-    return [(lo, min(CHUNK, rows - lo)) for lo in range(0, rows, CHUNK)]
+    starts = [lo for lo in STEPS if lo < rows]
+    return list(zip(starts, [hi - lo for lo, hi in zip(starts, starts[1:] + [rows])]))
 
 
 def block_plan(far, reach):
@@ -44,6 +45,10 @@
             places[(copy,) + key] = at
             at += 1
     return order, places, spans, at
+
+
+def pass_ends(last, near):
+    return (near + 2, last - 2, last)
 
 
 def moe_kernel(
@@ -215,25 +220,32 @@
         half = wg.shape[3]
         tile = min(256, half)
         width = x_ref.shape[1]
-
-        @pl.loop(0, 2)
-        def _(part):
-            for lo in range(0, half, tile):
-                x = x_ref[here, :]
-                a = jnp.dot(x, wg[copy, part, :, lo:lo + tile], preferred_element_type=jnp.float32)
-                u = jnp.dot(x, wu[copy, part, :, lo:lo + tile], preferred_element_type=jnp.float32)
-                h_ref[part, pl.ds(0, rows), lo:lo + tile] = (
-                    (a / (1.0 + jnp.exp(-a))) * u
-                ).astype(jnp.bfloat16)
-
         cols = min(512, width)
 
-        @pl.loop(0, width // cols)
-        def _(c):
-            at = pl.ds(pl.multiple_of(c * cols, cols), cols)
+        def widen(part, lo):
+            x = x_ref[here, :]
+            a = jnp.dot(x, wg[copy, part, :, lo:lo + tile], preferred_element_type=jnp.float32)
+            u = jnp.dot(x, wu[copy, part, :, lo:lo + tile], preferred_element_type=jnp.float32)
+            h_ref[part, pl.ds(0, rows), lo:lo + tile] = (
+                (a / (1.0 + jnp.exp(-a))) * u
+            ).astype(jnp.bfloat16)
+
+        def narrow(lo):
+            at = slice(lo, lo + cols)
             o = jnp.dot(h_ref[0, pl.ds(0, rows), :], wd[copy, 0, :, at], preferred_element_type=jnp.float32)
             o = o + jnp.dot(h_ref[1, pl.ds(0, rows), :], wd[copy, 1, :, at], preferred_element_type=jnp.float32)
             x_ref[here, at] = (o * wj_ref[here, 0:1]).astype(jnp.bfloat16)
+
+        return [
+            functools.partial(widen, part, lo) for part in (0, 1) for lo in range(0, half, tile)
+        ] + [functools.partial(narrow, lo) for lo in range(0, width, cols)]
+
+    work = []
+
+    def run(count):
+        for piece in work[:count]:
+            piece()
+        del work[:count]
 
     def upto(copy, d):
         return len([1 for key in order[copy] if key[1] <= d])
@@ -268,7 +280,7 @@
                     side_copy(j, copy, step, g).wait_send()
 
     select(0, 0)
-    mid = (last + near + 1) // 2
+    cuts = pass_ends(last, near)
     spread_weights()
     for d in range(1, last + 1):
         if d >= 3:
@@ -285,21 +297,23 @@
                 ring_copy(way, d - 1, i, lo, n).wait_recv()
                 if lo in onwards:
                     ring_copy(way, d, i, lo, onwards[lo]).start()
+            run(2)
         for way in (0, 1):
             select(way, d)
         if d == near:
             for j in range(3):
                 own_weight(j).wait()
                 pair_copy(j, 0).wait()
-            ffn(0, 0, upto(0, near))
+            work.extend(ffn(0, 0, upto(0, near)))
+        if d == near + 1:
             pair_weights()
-        if d == mid:
-            finish_weights()
-            ffn(1, 0, upto(1, mid))
-        if d == mid + 1:
-            ffn(2, 0, upto(2, mid + 1))
-    ffn(1, upto(1, mid), upto(1, last))
-    ffn(2, upto(2, mid + 1), upto(2, last))
+        if d in cuts:
+            if d == cuts[0]:
+                finish_weights()
+            before = max([-1] + [cut for cut in cuts if cut < d])
+            for copy in (1, 2):
+                work.extend(ffn(copy, upto(copy, before), upto(copy, d)))
+    run(len(work))
     for d in (last - 2, last - 1):
         for way in (0, 1):
             ring_copy(way, d, 0, 0, sizes[d + 1]).wait_send()
@@ -371,15 +385,16 @@
     offs, at = ([0] * (last + 2), 0)
     for d in range(1, last + 2):
         offs[d] = at
-        at += sizes[d]
+        at += -(-sizes[d] // 16) * 16
     total = at
     shared = last - 4
     half = w_gate.shape[2]
     block = -(-slots // 16) * 16
     order, places, spans, blocks = block_plan(far, REACH)
-    mid = (last + near + 1) // 2
+    marks = [-1] + list(pass_ends(last, near))
     widest = max(
-        len([1 for key in order[1] if key[1] <= mid]), len([1 for key in order[2] if key[1] <= mid + 1])
+        len([1 for key in order[copy] if lo < key[1] <= hi])
+        for copy in (0, 1, 2) for lo, hi in zip(marks, marks[1:])
     )
 
     z = lax.axis_index("ep")

time: 511 us -> 500 us (0.978)
  Pallas kernels: 497 us -> 486 us
    pallas_call x1, Pallas kernels: 497 us -> 486 us  [per_device(): call(jnp.stack(sorted_rows), jnp.stack(tables), sorted_own, own_table, jn...]
where the time goes in v3:
time: 500 us
  Pallas kernels  486 us (97%)
  other arithmetic  6.3 us (1%)
    pallas_call x1, Pallas kernels, per_device(): call(jnp.stack(sorted_rows), jnp.stack(tables), sorted_own, own_table, jn...  486 us

profile of v3, /device:TPU:46, one launch (start us, length us, event | category | flops | bytes accessed | tf_op | source)
XLA Modules:
  0.0 500.0 jit_solution(15449167873959678910)
XLA Ops:
  0.0 0.0 copy-start
  0.0 0.0 copy-start.1
  0.0 1.6 fusion.2
  1.6 0.8 copy.11
  2.4 0.1 eq.84
  2.6 0.3 fusion.5
  2.9 0.1 convert_element_type.56
  3.0 0.1 copy.12
  3.1 0.7 fusion.21
  3.8 0.3 convert_reduce_fusion
  4.1 1.8 fusion.1
  5.9 0.0 copy-done
  6.0 0.0 copy-done.1
  6.0 0.6 fusion
  6.6 0.0 copy-start.2
  6.6 0.0 copy-start.3
  6.6 1.5 pad_maximum_fusion.s_ref
  8.1 0.0 copy-done.2
  8.2 0.0 copy-done.3
  8.2 0.2 convolution_bitcast_fusion
  8.4 0.1 concatenate.10
  8.5 0.2 fusion.8
  8.7 0.6 fusion.25
  9.3 0.6 pad_maximum_fusion.1.meta_ref
  9.9 0.6 pad_maximum_fusion.2.own_ref
  10.6 0.1 iota_compare_fusion.2
  10.7 0.1 iota_compare_fusion.3
  10.8 0.7 add_convert_fusion.back_ref
  11.5 486.2 %shard_map.73 = bf16[256,2048]{1,0:T(8,128)(2,1)} custom-call(bf16[2,256,2048]{2,1,0:T(8,128)(2,1)} %pad_maximum_fusion.s_ref, f32[2,8,256]{2,1,0:T(8,128)} %pad_maximum_fusion.1.meta_ref, f32[8,256]{1,0:T(8,128)} %get-tuple-element.9.sorted_own_ref, f32[8,256]{1,0:T(8,128)} %pad_maximum_fusion.2.own_ref, bf16[2,256,256]{2,1,0:T(8,128)(2,1)} %add_convert_fusion.back_ref, ...), custom_call_target="tpu_custom_call" | custom-call | flops 6442450944 | bytes 25165824 | tf_op jit(solution)/shard_map/pallas_call | solution.py:485
  497.7 2.3 copy.15
  (5 shorter events, 0.0 us)
Async XLA Ops:
  0.0 5.9 %copy-start = (bf16[256,2048]{1,0:T(8,128)(2,1)S(1)}, bf16[256,2048]{1,0:T(8,128)(2,1)}, u32[]{:S(2)}) copy-start(bf16[256,2048]{1,0:T(8,128)(2,1)} %param.7) | copy-start | bytes 3145732
  0.0 6.0 %copy-start.1 = (f32[2048]{0:T(1024)S(1)}, f32[2048]{0:T(1024)}, u32[]{:S(2)}) copy-start(f32[2048]{0:T(1024)} %param.8) | copy-start | bytes 24580
  6.6 1.6 copy-start.2
  6.6 1.6 copy-start.3

commit v4 on v3

--- a/solution.py
+++ b/solution.py
@@ -53,12 +53,12 @@
 
 def moe_kernel(
     ring, groups, slots, sizes, offs, shared,
-    s_ref, meta_ref, sorted_own_ref, own_ref, back_ref, wg_hbm, wu_hbm, wd_hbm,
+    tok_hbm, gain_ref, ids_ref, route_ref, wg_hbm, wu_hbm, wd_hbm,
     out_ref,
-    held, meta_held, coming, final, contrib, x_ref, h_ref, wj_ref,
+    s_ref, meta_ref, sorted_own_ref, own_ref, table_ref, back_ref, held, meta_held, coming, final, contrib, x_ref, h_ref, wj_ref,
     wg, wu, wd,
     d_send, d_recv, m_send, m_recv, r_send, r_recv,
-    own_local, pair_send, pair_recv, far_send, far_recv, side_send, side_recv,
+    tok_local, own_local, pair_send, pair_recv, far_send, far_recv, side_send, side_recv,
 ):
     g = lax.axis_index("grp")
     z = lax.axis_index("ep")
@@ -75,6 +75,8 @@
     block = -(-slots // 16) * 16
     order, places, spans, _ = block_plan(far, REACH)
 
+    tokens_in = pltpu.make_async_copy(tok_hbm, x_ref.at[pl.ds(0, out_ref.shape[0])], tok_local)
+    tokens_in.start()
     barrier = pltpu.get_barrier_semaphore()
     for there in (up, down, far_up, far_down):
         pl.semaphore_signal(barrier, inc=1, device_id={"ep": there}, device_id_type=MESH)
@@ -172,17 +174,82 @@
             device_id_type=MESH,
         )
 
-    for way in (0, 1):
-        meta_copy(way, 0).start()
     for j in range(3):
         for copy in (1, 2):
             far_copy(j, copy).start()
-    for i, (lo, n) in enumerate(chunks_of(sizes[1])):
-        for way in (0, 1):
-            ring_copy(way, 0, i, lo, n).start()
     for j in range(3):
         own_weight(j).start()
         pair_copy(j, 0).start()
+
+    tok = out_ref.shape[0]
+    tokens_in.wait()
+    step = min(64, tok)
+
+    @pl.loop(0, tok // step)
+    def _(i):
+        at = pl.ds(pl.multiple_of(i * step, step), step)
+        values = x_ref[at, :].astype(jnp.float32)
+        scale = lax.rsqrt(jnp.mean(values * values, axis=-1, keepdims=True) + 1e-06)
+        contrib[0, at, :] = (values * scale * gain_ref[...]).astype(jnp.bfloat16)
+
+    down_at = lax.broadcasted_iota(jnp.int32, (tok, tok), 0)
+    across_at = lax.broadcasted_iota(jnp.int32, (tok, tok), 1)
+    before_it = down_at < across_at
+
+    def column(row):
+        return jnp.sum(jnp.where(down_at == across_at, row, 0.0), axis=1, keepdims=True)
+
+    def count_down(test):
+        return jnp.sum(jnp.where(test, 1.0, 0.0), axis=0, keepdims=True)
+
+    ids = [ids_ref[k:k + 1, :].astype(jnp.float32) for k in (0, 1)]
+    routes = [route_ref[k:k + 1, :] for k in (0, 1)]
+    id_columns = [column(row) for row in ids]
+    hosts, targets = ([], [])
+    for k in (0, 1):
+        named = (id_columns[0] == ids[k]) | (id_columns[1] == ids[k])
+        slot = count_down(named & before_it)
+        targets.append(ids[k] * slots + slot)
+        off = ids[k] - z.astype(jnp.float32)
+        off = jnp.where(off < 0.0, off + ring, off)
+        ahead_half = (off < far) | ((off == far) & (slot < slots // 2))
+        signed = jnp.where(ahead_half, off, off - ring)
+        hosts.append(
+            jnp.where(
+                jnp.abs(signed) <= near, signed,
+                jnp.where(signed > 0.0, signed - REACH, signed + REACH),
+            )
+        )
+    own_ref[...] = jnp.zeros_like(own_ref)
+    for k in (0, 1):
+        own_ref[k:k + 1, :] = jnp.where(hosts[k] == 0.0, targets[k], -1.0)
+        own_ref[2 + k:3 + k, :] = routes[k]
+    for way in (0, 1):
+        dist = [host if way == 0 else -host for host in hosts]
+        reach = jnp.maximum(jnp.maximum(dist[0], dist[1]), 0.0)
+        reach_column = column(reach)
+        place = count_down((reach_column > reach) | ((reach_column == reach) & before_it))
+        back = jnp.where(column(place) == across_at.astype(jnp.float32), 1.0, 0.0)
+        back_ref[way] = back.astype(jnp.bfloat16)
+        table = table_ref
+        table[...] = jnp.zeros_like(own_ref)
+        for k in (0, 1):
+            table[k:k + 1, :] = jnp.where(dist[k] > 0.0, targets[k], -1.0)
+            table[2 + k:3 + k, :] = routes[k]
+        meta_ref[way] = jnp.dot(
+            table[...], back, precision=lax.Precision.HIGHEST, preferred_element_type=jnp.float32
+        )
+        if way == 0:
+            sorted_own_ref[...] = jnp.dot(
+                own_ref[...], back, precision=lax.Precision.HIGHEST, preferred_element_type=jnp.float32
+            )
+        pick = jnp.where(place == down_at.astype(jnp.float32), 1.0, 0.0).astype(jnp.bfloat16)
+        s_ref[way] = jnp.dot(
+            pick, contrib[0], preferred_element_type=jnp.float32
+        ).astype(jnp.bfloat16)
+        meta_copy(way, 0).start()
+        for i, (lo, n) in enumerate(chunks_of(sizes[1])):
+            ring_copy(way, 0, i, lo, n).start()
 
     slot_row = lax.broadcasted_iota(jnp.int32, (block, 1), 0).astype(jnp.float32)
     wanted = tuple(
@@ -397,49 +464,6 @@
         for copy in (0, 1, 2) for lo, hi in zip(marks, marks[1:])
     )
 
-    z = lax.axis_index("ep")
-    values = tokens.astype(jnp.float32)
-    scale = lax.rsqrt(jnp.mean(values * values, axis=-1, keepdims=True) + 1e-06)
-    normed = (values * scale * norm_gain).astype(jnp.bfloat16)
-
-    flat = expert_ids.reshape(-1)
-    onehot = (flat[:, None] == jnp.arange(experts, dtype=jnp.int32)[None, :]).astype(jnp.bfloat16)
-    count = tok * top
-    earlier = (jnp.arange(count)[:, None] > jnp.arange(count)[None, :]).astype(jnp.bfloat16)
-    before = jnp.dot(earlier, onehot, preferred_element_type=jnp.float32)
-    slot = jnp.sum(before * onehot.astype(jnp.float32), axis=1).astype(jnp.int32).reshape(tok, top)
-    target = (expert_ids * slots + slot).astype(jnp.float32)
-    off = lax.rem(expert_ids - z + ring, ring)
-    ahead_half = (off < far) | ((off == far) & (slot < slots // 2))
-    signed = jnp.where(ahead_half, off, off - ring)
-    host = jnp.where(
-        jnp.abs(signed) <= near, signed, jnp.where(signed > 0, signed - REACH, signed + REACH)
-    )
-    extra = [route_weights.T, jnp.zeros((4, tok), jnp.float32)]
-    own_table = jnp.concatenate([jnp.where(host == 0, target, -1.0).T] + extra)
-    tables, backs, sorted_rows = ([], [], [])
-    for dist in (host, -host):
-        reach = jnp.max(jnp.maximum(dist, 0), axis=1)
-        ahead = (reach[None, :] > reach[:, None]) | (
-            (reach[None, :] == reach[:, None])
-            & (jnp.arange(tok)[None, :] < jnp.arange(tok)[:, None])
-        )
-        place = jnp.sum(ahead.astype(jnp.int32), axis=1)
-        back = (place[:, None] == jnp.arange(tok)[None, :])
-        table = jnp.concatenate([jnp.where(dist > 0, target, -1.0).T] + extra)
-        if not tables:
-            table = jnp.concatenate([table, own_table])
-        tables.append(jnp.dot(table, back.astype(jnp.float32), precision=lax.Precision.HIGHEST))
-        back = back.astype(jnp.bfloat16)
-        backs.append(back)
-        sorted_rows.append(
-            lax.dot_general(
-                back, normed, (((0,), (0,)), ((), ())), preferred_element_type=jnp.float32
-            ).astype(jnp.bfloat16)
-        )
-    sorted_own = tables[0][8:]
-    tables[0] = tables[0][:8]
-
     vm = pl.BlockSpec(memory_space=pltpu.VMEM)
     hbm = pl.BlockSpec(memory_space=pl.ANY)
     most = len(chunks_of(tok))
@@ -447,9 +471,15 @@
     call = pl.pallas_call(
         functools.partial(moe_kernel, ring, groups, slots, sizes, offs, shared),
         out_shape=jax.ShapeDtypeStruct((tok, width), bf16),
-        in_specs=[vm, vm, vm, vm, vm, hbm, hbm, hbm],
+        in_specs=[hbm, vm, vm, vm, hbm, hbm, hbm],
         out_specs=vm,
         scratch_shapes=[
+            pltpu.VMEM((2, tok, width), bf16),
+            pltpu.VMEM((2, 8, tok), f32),
+            pltpu.VMEM((8, tok), f32),
+            pltpu.VMEM((8, tok), f32),
+            pltpu.VMEM((8, tok), f32),
+            pltpu.VMEM((2, tok, tok), bf16),
             pltpu.VMEM((2, total, width), bf16),
             pltpu.VMEM((2, last, 8, tok), f32),
             pltpu.VMEM((2, total - offs[shared + 1], width), bf16),
@@ -467,6 +497,7 @@
             pltpu.SemaphoreType.DMA((2, last)),
             pltpu.SemaphoreType.DMA((2, last)),
             pltpu.SemaphoreType.DMA((2, last, most)),
+            pltpu.SemaphoreType.DMA,
             pltpu.SemaphoreType.DMA((3,)),
             pltpu.SemaphoreType.DMA((3, 3)),
             pltpu.SemaphoreType.DMA((3, 3)),
@@ -483,7 +514,7 @@
         ),
     )
     return call(
-        jnp.stack(sorted_rows), jnp.stack(tables), sorted_own, own_table, jnp.stack(backs),
+        tokens, norm_gain.reshape(1, width), expert_ids.T, route_weights.T,
         w_gate, w_up, w_down,
     )
 

time: 500 us -> 487 us (0.974)
  other arithmetic: 6.3 us -> 0 us
where the time goes in v4:
time: 487 us
  Pallas kernels  485 us (100%)
    pallas_call x1, Pallas kernels, per_device(): call(tokens, norm_gain.reshape(1, width), expert_ids.T, route_weights.T,...  485 us

profile of v4, /device:TPU:46, one launch (start us, length us, event | category | flops | bytes accessed | tf_op | source)
XLA Modules:
  0.0 487.1 jit_solution(14335976101906604902)
XLA Ops:
  0.0 484.8 %shard_map.73 = bf16[256,2048]{1,0:T(8,128)(2,1)} custom-call(bf16[256,2048]{1,0:T(8,128)(2,1)} %tok_hbm.1, f32[1,2048]{1,0:T(1,128)} %bitcast.3, s32[2,256]{1,0:T(2,128)} %bitcast.4, f32[2,256]{1,0:T(2,128)} %bitcast.5, bf16[1,2048,512]{2,1,0:T(8,128)(2,1)} %wg_hbm.1, bf16[1,2048,512]{2,1,0:T(8,128)(2,1)} %wu_hbm.1, bf16[1,512,2048]{2,1,0:T(8,128)(2,1)} %wd_hbm.1), custom_call_target="tpu_custom_call" | custom-call | flops 6442450944 | bytes 25165824 | tf_op jit(solution)/shard_map/pallas_call | solution.py:516
  484.8 2.3 copy.9

commit v5 on v4

--- a/solution.py
+++ b/solution.py
@@ -12,12 +12,18 @@
 REACH = 5
 
 
-def prefix_sizes(tok, slots, far, reach):
+def opposite_split(slots):
+    return -(-slots // 16) * 8
+
+
+def prefix_sizes(tok, slots, far, reach, way):
+    first = opposite_split(slots)
+    at_far = first if way == 0 else slots - first
     last = far - reach
     near = reach // 2
     sizes = [0] * (last + 2)
     for d in range(1, last + 1):
-        rows = slots * (last - d) + slots // 2 + 2 * slots * max(0, near - d + 1)
+        rows = slots * (last - d) + at_far + 2 * slots * max(0, near - d + 1)
         sizes[d] = -(-min(tok, rows) // 8) * 8
     return sizes
 
@@ -48,7 +54,7 @@
 
 
 def pass_ends(last, near):
-    return (near + 2, last - 2, last)
+    return (near + 2, last - 3, last)
 
 
 def moe_kernel(
@@ -66,10 +72,11 @@
     far = ring // 2
     last = far - REACH
     near = REACH // 2
-    up = lax.rem(z + 1, ring)
-    down = lax.rem(z + ring - 1, ring)
-    far_up = lax.rem(z + REACH, ring)
-    far_down = lax.rem(z + ring - REACH, ring)
+    turn = 1 - 2 * core
+    up = lax.rem(z + ring + turn, ring)
+    down = lax.rem(z + ring - turn, ring)
+    far_up = lax.rem(z + ring + turn * REACH, ring)
+    far_down = lax.rem(z + ring - turn * REACH, ring)
     onward = (up, down)
     home = (down, up)
     block = -(-slots // 16) * 16
@@ -119,11 +126,12 @@
 
     def pair_copy(j, copy):
         src, dst = weights[j]
+        there = (0, 2, 1)[copy]
         return pltpu.make_async_remote_copy(
             src_ref=src.at[0] if copy == 0 else dst.at[copy, 0],
-            dst_ref=dst.at[copy, 1],
+            dst_ref=dst.at[there, 1],
             send_sem=pair_send.at[copy, j],
-            recv_sem=pair_recv.at[copy, j],
+            recv_sem=pair_recv.at[there, j],
             device_id={"tp": 1 - core},
             device_id_type=MESH,
         )
@@ -132,15 +140,23 @@
         src, dst = weights[j]
         return pltpu.make_async_copy(src.at[0], dst.at[0, 0], own_local.at[j])
 
+    def both_ways(d):
+        lists = [chunks_of(sizes[way][d]) for way in (0, 1)]
+        return [
+            (i, way) + lists[way][i]
+            for i in range(max(len(rows) for rows in lists))
+            for way in (0, 1) if i < len(lists[way])
+        ]
+
     def rows_out(way, d, lo, n):
         if d == 0:
             return s_ref.at[way, pl.ds(lo, n)]
-        return held.at[way, pl.ds(offs[d] + lo, n)]
+        return held.at[way, pl.ds(offs[way][d] + lo, n)]
 
     def ring_copy(way, d, i, lo, n):
         return pltpu.make_async_remote_copy(
             src_ref=rows_out(way, d, lo, n),
-            dst_ref=held.at[way, pl.ds(offs[d + 1] + lo, n)],
+            dst_ref=held.at[way, pl.ds(offs[way][d + 1] + lo, n)],
             send_sem=d_send.at[way, d],
             recv_sem=d_recv.at[way, d, i],
             device_id={"ep": onward[way]},
@@ -161,8 +177,8 @@
         if d == 0:
             return final.at[way, pl.ds(lo, n)]
         if d <= shared:
-            return held.at[way, pl.ds(offs[d] + lo, n)]
-        return coming.at[way, pl.ds(offs[d] - offs[shared + 1] + lo, n)]
+            return held.at[way, pl.ds(offs[way][d] + lo, n)]
+        return coming.at[way, pl.ds(offs[way][d] - offs[way][shared + 1] + lo, n)]
 
     def home_copy(way, d, i, lo, n):
         return pltpu.make_async_remote_copy(
@@ -210,9 +226,9 @@
         named = (id_columns[0] == ids[k]) | (id_columns[1] == ids[k])
         slot = count_down(named & before_it)
         targets.append(ids[k] * slots + slot)
-        off = ids[k] - z.astype(jnp.float32)
+        off = (ids[k] - z.astype(jnp.float32)) * turn.astype(jnp.float32)
         off = jnp.where(off < 0.0, off + ring, off)
-        ahead_half = (off < far) | ((off == far) & (slot < slots // 2))
+        ahead_half = (off < far) | ((off == far) & (slot < opposite_split(slots)))
         signed = jnp.where(ahead_half, off, off - ring)
         hosts.append(
             jnp.where(
@@ -248,7 +264,7 @@
             pick, contrib[0], preferred_element_type=jnp.float32
         ).astype(jnp.bfloat16)
         meta_copy(way, 0).start()
-        for i, (lo, n) in enumerate(chunks_of(sizes[1])):
+        for i, (lo, n) in enumerate(chunks_of(sizes[way][1])):
             ring_copy(way, 0, i, lo, n).start()
 
     slot_row = lax.broadcasted_iota(jnp.int32, (block, 1), 0).astype(jnp.float32)
@@ -266,7 +282,7 @@
         return sorted_own_ref[...] if d == 0 else meta_held[way, d - 1]
 
     def select(way, d):
-        rows = s_ref.shape[1] if d == 0 else sizes[d]
+        rows = s_ref.shape[1] if d == 0 else sizes[way][d]
         table = table_of(way, d)
         for copy in (0, 1, 2):
             if (copy, way, d) not in places:
@@ -275,7 +291,7 @@
             a, b = matches(table, copy)
             scale = jnp.sum(a * table[2:3, :] + b * table[3:4, :], axis=1, keepdims=True)
             one = (a + b).astype(jnp.bfloat16)[:, :rows]
-            source = s_ref[0] if d == 0 else held[way, pl.ds(offs[d], rows)]
+            source = s_ref[0] if d == 0 else held[way, pl.ds(offs[way][d], rows)]
             got = jnp.dot(one, source, preferred_element_type=jnp.float32)
             x_ref[at, :] = got.astype(jnp.bfloat16)
             wj_ref[at, :] = jnp.broadcast_to(scale, (block, wj_ref.shape[1]))
@@ -352,19 +368,19 @@
     for d in range(1, last + 1):
         if d >= 3:
             for way in (0, 1):
-                ring_copy(way, d - 3, 0, 0, sizes[d - 2]).wait_send()
+                ring_copy(way, d - 3, 0, 0, sizes[way][d - 2]).wait_send()
                 meta_copy(way, d - 3).wait_send()
         for way in (0, 1):
             meta_copy(way, d - 1).wait_recv()
             if d < last:
                 meta_copy(way, d).start()
-        onwards = dict((lo, n) for lo, n in chunks_of(sizes[d + 1])) if d < last else {}
-        for i, (lo, n) in enumerate(chunks_of(sizes[d])):
-            for way in (0, 1):
-                ring_copy(way, d - 1, i, lo, n).wait_recv()
-                if lo in onwards:
-                    ring_copy(way, d, i, lo, onwards[lo]).start()
-            run(2)
+        onwards = [dict(chunks_of(sizes[way][d + 1])) for way in (0, 1)]
+        for i, way, lo, n in both_ways(d):
+            ring_copy(way, d - 1, i, lo, n).wait_recv()
+            if lo in onwards[way]:
+                ring_copy(way, d, i, lo, onwards[way][lo]).start()
+            if way == 1:
+                run(3 if d > cuts[1] else 2)
         for way in (0, 1):
             select(way, d)
         if d == near:
@@ -383,7 +399,7 @@
     run(len(work))
     for d in (last - 2, last - 1):
         for way in (0, 1):
-            ring_copy(way, d, 0, 0, sizes[d + 1]).wait_send()
+            ring_copy(way, d, 0, 0, sizes[way][d + 1]).wait_send()
             meta_copy(way, d).wait_send()
 
     def gathered(table, rows, way, d, at):
@@ -402,25 +418,22 @@
 
     for d in range(last, 0, -1):
         for way in (0, 1):
-            got = gathered(meta_held[way, d - 1], sizes[d], way, d, slice(None))
-            contrib[way, pl.ds(0, sizes[d])] = got.astype(jnp.bfloat16)
-        arriving = dict((lo, n) for lo, n in chunks_of(sizes[d + 1])) if d < last else {}
-        for i, (lo, n) in enumerate(chunks_of(sizes[d])):
-            for way in (0, 1):
-                m = arriving.get(lo, 0)
-                if m:
-                    home_copy(way, d + 1, i, lo, m).wait_recv()
-                    was = inbox(way, d, lo, m)
-                    was[...] = (
-                        was[...].astype(jnp.float32)
-                        + contrib[way, pl.ds(lo, m)].astype(jnp.float32)
-                    ).astype(jnp.bfloat16)
-                if m < n:
-                    inbox(way, d, lo + m, n - m)[...] = contrib[way, pl.ds(lo + m, n - m)]
-                home_copy(way, d, i, lo, n).start()
-    for i, (lo, n) in enumerate(chunks_of(sizes[1])):
-        for way in (0, 1):
-            home_copy(way, 1, i, lo, n).wait_recv()
+            got = gathered(meta_held[way, d - 1], sizes[way][d], way, d, slice(None))
+            contrib[way, pl.ds(0, sizes[way][d])] = got.astype(jnp.bfloat16)
+        arriving = [dict(chunks_of(sizes[way][d + 1])) for way in (0, 1)]
+        for i, way, lo, n in both_ways(d):
+            m = arriving[way].get(lo, 0)
+            if m:
+                home_copy(way, d + 1, i, lo, m).wait_recv()
+                was = inbox(way, d, lo, m)
+                was[...] = (
+                    was[...].astype(jnp.float32) + contrib[way, pl.ds(lo, m)].astype(jnp.float32)
+                ).astype(jnp.bfloat16)
+            if m < n:
+                inbox(way, d, lo + m, n - m)[...] = contrib[way, pl.ds(lo + m, n - m)]
+            home_copy(way, d, i, lo, n).start()
+    for i, way, lo, n in both_ways(1):
+        home_copy(way, 1, i, lo, n).wait_recv()
 
     tok, width = out_ref.shape
     cols = min(512, width)
@@ -435,7 +448,7 @@
 
     for d in range(last, 0, -1):
         for way in (0, 1):
-            home_copy(way, d, 0, 0, sizes[d]).wait_send()
+            home_copy(way, d, 0, 0, sizes[way][d]).wait_send()
 
 
 def per_device(tokens, norm_gain, expert_ids, route_weights, w_gate, w_up, w_down):
@@ -448,12 +461,13 @@
     far = ring // 2
     last = far - REACH
     near = REACH // 2
-    sizes = prefix_sizes(tok, slots, far, REACH)
-    offs, at = ([0] * (last + 2), 0)
-    for d in range(1, last + 2):
-        offs[d] = at
-        at += -(-sizes[d] // 16) * 16
-    total = at
+    sizes = [prefix_sizes(tok, slots, far, REACH, way) for way in (0, 1)]
+    offs = [[0] * (last + 2), [0] * (last + 2)]
+    for way in (0, 1):
+        for d in range(1, last + 1):
+            offs[way][d + 1] = offs[way][d] + -(-sizes[way][d] // 16) * 16
+    total = max(offs[0][last + 1], offs[1][last + 1])
+    late = max(offs[way][last + 1] - offs[way][last - 3] for way in (0, 1))
     shared = last - 4
     half = w_gate.shape[2]
     block = -(-slots // 16) * 16
@@ -482,7 +496,7 @@
             pltpu.VMEM((2, tok, tok), bf16),
             pltpu.VMEM((2, total, width), bf16),
             pltpu.VMEM((2, last, 8, tok), f32),
-            pltpu.VMEM((2, total - offs[shared + 1], width), bf16),
+            pltpu.VMEM((2, late, width), bf16),
             pltpu.VMEM((2, tok, width), bf16),
             pltpu.VMEM((2, tok, width), bf16),
             pltpu.VMEM((blocks * block, width), bf16),

time: 487 us -> 481 us (0.988)
  Pallas kernels: 485 us -> 477 us
    pallas_call x1, Pallas kernels: 485 us -> 477 us  [per_device(): call(tokens, norm_gain.reshape(1, width), expert_ids.T, route_weights.T,...]
where the time goes in v5:
time: 481 us; the launch traced here: 479 us
  Pallas kernels  477 us (99%)
    pallas_call x1, Pallas kernels, per_device(): call(tokens, norm_gain.reshape(1, width), expert_ids.T, route_weights.T,...  477 us

profile of v5, /device:TPU:46, one launch (start us, length us, event | category | flops | bytes accessed | tf_op | source)
XLA Modules:
  0.0 479.1 jit_solution(10661472815208528974)
XLA Ops:
  0.0 476.8 %shard_map.73 = bf16[256,2048]{1,0:T(8,128)(2,1)} custom-call(bf16[256,2048]{1,0:T(8,128)(2,1)} %tok_hbm.1, f32[1,2048]{1,0:T(1,128)} %bitcast.3, s32[2,256]{1,0:T(2,128)} %bitcast.4, f32[2,256]{1,0:T(2,128)} %bitcast.5, bf16[1,2048,512]{2,1,0:T(8,128)(2,1)} %wg_hbm.1, bf16[1,2048,512]{2,1,0:T(8,128)(2,1)} %wu_hbm.1, bf16[1,512,2048]{2,1,0:T(8,128)(2,1)} %wd_hbm.1), custom_call_target="tpu_custom_call" | custom-call | flops 6442450944 | bytes 25165824 | tf_op jit(solution)/shard_map/pallas_call | solution.py:530
  476.8 2.3 copy.9

commit v6 on v5

--- a/solution.py
+++ b/solution.py
@@ -9,6 +9,7 @@
 
 MESH = pl.DeviceIdType.MESH
 STEPS = (0, 16, 32, 64, 128, 192)
+LATE = STEPS[-1]
 REACH = 5
 
 
@@ -53,8 +54,12 @@
     return order, places, spans, at
 
 
-def pass_ends(last, near):
-    return (near + 2, last - 3, last)
+def late_reach(sizes):
+    return max(d for rows in sizes for d in range(1, len(rows)) if rows[d] > LATE)
+
+
+def pass_ends(last, late):
+    return (late + 3, last - 3, last)
 
 
 def moe_kernel(
@@ -265,7 +270,8 @@
         ).astype(jnp.bfloat16)
         meta_copy(way, 0).start()
         for i, (lo, n) in enumerate(chunks_of(sizes[way][1])):
-            ring_copy(way, 0, i, lo, n).start()
+            if lo < LATE:
+                ring_copy(way, 0, i, lo, n).start()
 
     slot_row = lax.broadcasted_iota(jnp.int32, (block, 1), 0).astype(jnp.float32)
     wanted = tuple(
@@ -363,12 +369,24 @@
                     side_copy(j, copy, step, g).wait_send()
 
     select(0, 0)
-    cuts = pass_ends(last, near)
+    late = late_reach(sizes)
+    cuts = pass_ends(last, late)
+
+    def late_rows(way, d):
+        return max(0, sizes[way][d] - LATE)
+
+    def late_hop(d):
+        for way in (0, 1):
+            if d > 0 and late_rows(way, d):
+                ring_copy(way, d - 1, STEPS.index(LATE), LATE, late_rows(way, d)).wait_recv()
+            if late_rows(way, d + 1):
+                ring_copy(way, d, STEPS.index(LATE), LATE, late_rows(way, d + 1)).start()
+
     spread_weights()
     for d in range(1, last + 1):
         if d >= 3:
             for way in (0, 1):
-                ring_copy(way, d - 3, 0, 0, sizes[way][d - 2]).wait_send()
+                ring_copy(way, d - 3, 0, 0, min(LATE, sizes[way][d - 2])).wait_send()
                 meta_copy(way, d - 3).wait_send()
         for way in (0, 1):
             meta_copy(way, d - 1).wait_recv()
@@ -376,26 +394,32 @@
                 meta_copy(way, d).start()
         onwards = [dict(chunks_of(sizes[way][d + 1])) for way in (0, 1)]
         for i, way, lo, n in both_ways(d):
+            if lo >= LATE:
+                continue
             ring_copy(way, d - 1, i, lo, n).wait_recv()
             if lo in onwards[way]:
                 ring_copy(way, d, i, lo, onwards[way][lo]).start()
             if way == 1:
                 run(3 if d > cuts[1] else 2)
-        for way in (0, 1):
-            select(way, d)
+        if d > late:
+            for way in (0, 1):
+                select(way, d)
         if d == near:
             for j in range(3):
                 own_weight(j).wait()
                 pair_copy(j, 0).wait()
-            work.extend(ffn(0, 0, upto(0, near)))
         if d == near + 1:
             pair_weights()
         if d in cuts:
             if d == cuts[0]:
                 finish_weights()
-            before = max([-1] + [cut for cut in cuts if cut < d])
+            before = max([late] + [cut for cut in cuts if cut < d])
             for copy in (1, 2):
                 work.extend(ffn(copy, upto(copy, before), upto(copy, d)))
+        if d == last - 1:
+            late_hop(0)
+    run(len(work) // 2)
+    late_hop(1)
     run(len(work))
     for d in (last - 2, last - 1):
         for way in (0, 1):
@@ -417,6 +441,10 @@
         return got
 
     for d in range(last, 0, -1):
+        if d == last - 5:
+            run(len(work) - rest)
+        if d == late:
+            run(len(work))
         for way in (0, 1):
             got = gathered(meta_held[way, d - 1], sizes[way][d], way, d, slice(None))
             contrib[way, pl.ds(0, sizes[way][d])] = got.astype(jnp.bfloat16)
@@ -432,6 +460,24 @@
             if m < n:
                 inbox(way, d, lo + m, n - m)[...] = contrib[way, pl.ds(lo + m, n - m)]
             home_copy(way, d, i, lo, n).start()
+            if way == 1:
+                run(2)
+        if d == last:
+            for hop in range(2, late):
+                late_hop(hop)
+        if d == last - 1:
+            late_hop(late)
+            for way in (0, 1):
+                for hop in range(0, late):
+                    if late_rows(way, hop + 1):
+                        ring_copy(way, hop, 0, LATE, late_rows(way, hop + 1)).wait_send()
+            for hop in range(1, late + 1):
+                work.extend(functools.partial(select, way, hop) for way in (0, 1))
+            final_passes = ffn(0, 0, upto(0, near))
+            for copy in (1, 2):
+                final_passes.extend(ffn(copy, 0, upto(copy, late)))
+            rest = len(final_passes)
+            work.extend(final_passes)
     for i, way, lo, n in both_ways(1):
         home_copy(way, 1, i, lo, n).wait_recv()
 
@@ -467,12 +513,13 @@
         for d in range(1, last + 1):
             offs[way][d + 1] = offs[way][d] + -(-sizes[way][d] // 16) * 16
     total = max(offs[0][last + 1], offs[1][last + 1])
-    late = max(offs[way][last + 1] - offs[way][last - 3] for way in (0, 1))
+    beyond = max(offs[way][last + 1] - offs[way][last - 3] for way in (0, 1))
     shared = last - 4
     half = w_gate.shape[2]
     block = -(-slots // 16) * 16
     order, places, spans, blocks = block_plan(far, REACH)
-    marks = [-1] + list(pass_ends(last, near))
+    late = late_reach(sizes)
+    marks = [-1, late] + list(pass_ends(last, late))
     widest = max(
         len([1 for key in order[copy] if lo < key[1] <= hi])
         for copy in (0, 1, 2) for lo, hi in zip(marks, marks[1:])
@@ -496,7 +543,7 @@
             pltpu.VMEM((2, tok, tok), bf16),
             pltpu.VMEM((2, total, width), bf16),
             pltpu.VMEM((2, last, 8, tok), f32),
-            pltpu.VMEM((2, late, width), bf16),
+            pltpu.VMEM((2, beyond, width), bf16),
             pltpu.VMEM((2, tok, width), bf16),
             pltpu.VMEM((2, tok, width), bf16),
             pltpu.VMEM((blocks * block, width), bf16),

time: 481 us -> 475 us (0.988)
  Pallas kernels: 477 us -> 472 us
    pallas_call x1, Pallas kernels: 477 us -> 472 us  [per_device(): call(tokens, norm_gain.reshape(1, width), expert_ids.T, route_weights.T,...]
where the time goes in v6:
time: 475 us; the launch traced here: 474 us
  Pallas kernels  472 us (99%)
    pallas_call x1, Pallas kernels, per_device(): call(tokens, norm_gain.reshape(1, width), expert_ids.T, route_weights.T,...  472 us

profile of v6, /device:TPU:46, one launch (start us, length us, event | category | flops | bytes accessed | tf_op | source)
XLA Modules:
  0.0 474.0 jit_solution(6368228952843850789)
XLA Ops:
  0.0 471.7 %shard_map.73 = bf16[256,2048]{1,0:T(8,128)(2,1)} custom-call(bf16[256,2048]{1,0:T(8,128)(2,1)} %tok_hbm.1, f32[1,2048]{1,0:T(1,128)} %bitcast.3, s32[2,256]{1,0:T(2,128)} %bitcast.4, f32[2,256]{1,0:T(2,128)} %bitcast.5, bf16[1,2048,512]{2,1,0:T(8,128)(2,1)} %wg_hbm.1, bf16[1,2048,512]{2,1,0:T(8,128)(2,1)} %wu_hbm.1, bf16[1,512,2048]{2,1,0:T(8,128)(2,1)} %wd_hbm.1), custom_call_target="tpu_custom_call" | custom-call | flops 6442450944 | bytes 25165824 | tf_op jit(solution)/shard_map/pallas_call | solution.py:577
  471.7 2.3 copy.9
